TPU v7x, 32 devices: a whole 2x2x4 slice. The times are simulated.
32 devices in a mesh: grp: 2 (over y), kv: 4 (over z), tp: 4 (over x, core).
Axes of the slice: x: 2, y: 2, z: 4, core: 2. Of those that a mesh axis runs over, the one named last changes fastest.
Arguments:
- tokens: bfloat16 [256, 4, 2048], P(('grp', 'kv'), None, 'tp'), parts along dimension 0, may hold values from -6 to 6
- in_gain: float32 [2048], replicated, may hold values from 0.1 to 1.9
- w_query: bfloat16 [2048, 1024], P('kv', 'tp'), may hold values from -0.125 to 0.125
- w_key: bfloat16 [2048, 1024], P('kv', 'tp'), may hold values from -0.125 to 0.125
- w_value: bfloat16 [2048, 1024], P('kv', 'tp'), may hold values from -0.125 to 0.125
- w_gate: bfloat16 [2048, 1024], P('kv', 'tp'), may hold values from -0.125 to 0.125
- w_beta: bfloat16 [2048, 16], replicated, may hold values from -0.125 to 0.125
- w_decay: bfloat16 [2048, 16], replicated, may hold values from -0.125 to 0.125
- decay_base: float32 [16], P('tp'), may hold values from 0.05 to 1
- out_gain: float32 [64], replicated, may hold values from 0.1 to 1.9
- w_out: bfloat16 [1024, 2048], P('tp', 'kv'), may hold values from -0.1875 to 0.1875
- state: float32 [256, 64, 1024], P(('grp', 'kv'), None, 'tp'), parts along dimension 0, may hold values from -0.8 to 0.8
- prev_keys: bfloat16 [256, 4, 1024], P(('grp', 'kv'), None, 'tp'), parts along dimension 0, may hold values from -6 to 6
- prev_values: bfloat16 [256, 4, 1024], P(('grp', 'kv'), None, 'tp'), parts along dimension 0, may hold values from -6 to 6
- prev_beta: float32 [256, 4, 16], P(('grp', 'kv'), None, 'tp'), parts along dimension 0, may hold values from -6 to 6
- prev_decay: float32 [256, 4, 16], P(('grp', 'kv'), None, 'tp'), parts along dimension 0, may hold values from -1 to -0.02
- accepted: int32 [256], P(('grp', 'kv')), parts along dimension 0, may hold values from 0 to 4
Outputs:
- mixed: bfloat16 [256, 4, 2048], P(('grp', 'kv'), None, 'tp'), parts along dimension 0
- new_state: float32 [256, 64, 1024], P(('grp', 'kv'), None, 'tp'), parts along dimension 0
There are 2 independent parts, one for each index of `grp`. A program takes and returns all parts, laid end to end along the dimension named above; an argument that names none is the same for every part. Nothing has to cross between parts.
All inputs are finite; a program needn't handle non-finite values.
Results may differ from a plain program's by a relative error of at most 0.012.
Values may be sent and summed in bfloat16 or wider, within the bound.
A program may use at most 128 MiB of HBM per device.

v0:
```python
import jax
import jax.numpy as jnp
from jax import lax
from jax.sharding import PartitionSpec as P

EPS = 1e-06


def normalize_rows(vector):
    return vector * lax.rsqrt(jnp.sum(vector * vector, -1, keepdims=True) + EPS)


def delta_block(saved, queries, keys_in, values_in, strength, log_decay):
    highest = lax.Precision.HIGHEST
    steps_len = queries.shape[1]
    cumul = jnp.transpose(jnp.cumsum(log_decay, axis=1), (0, 2, 1))
    q_heads = jnp.transpose(queries, (0, 2, 1, 3))
    k_heads = jnp.transpose(keys_in, (0, 2, 1, 3))
    v_heads = jnp.transpose(values_in, (0, 2, 1, 3))
    weight_t = jnp.transpose(strength, (0, 2, 1))
    spread = cumul[..., :, None] - cumul[..., None, :]
    order = jnp.arange(steps_len)
    inside = order[:, None] >= order[None, :]
    below = order[:, None] > order[None, :]
    dec_incl = jnp.where(inside, jnp.exp(jnp.where(inside, spread, 0.0)), 0.0)
    dec_strict = jnp.where(below, dec_incl, 0.0)
    lower_mat = (
        weight_t[..., :, None]
        * jnp.einsum("bhik,bhjk->bhij", k_heads, k_heads, precision=highest)
        * dec_strict
    )
    growth = jnp.exp(cumul)
    rhs_all = jnp.concatenate(
        [weight_t[..., None] * v_heads, (weight_t * growth)[..., None] * k_heads], axis=-1
    )
    solved = []
    for row_index in range(steps_len):
        current = rhs_all[:, :, row_index]
        for col_index in range(row_index):
            current = current - lower_mat[:, :, row_index, col_index, None] * solved[col_index]
        solved.append(current)
    solution = jnp.stack(solved, axis=2)
    value_size = v_heads.shape[-1]
    update = solution[..., :value_size] - jnp.einsum(
        "bhpk,bhkv->bhpv", solution[..., value_size:], saved, precision=highest
    )
    scores = jnp.einsum("bhik,bhjk->bhij", q_heads, k_heads, precision=highest) * dec_incl
    output = jnp.einsum(
        "bhpk,bhkv->bhpv", growth[..., None] * q_heads, saved, precision=highest
    ) + jnp.einsum("bhij,bhjv->bhiv", scores, update, precision=highest)
    tail = jnp.exp(cumul[..., -1:] - cumul)[..., None] * k_heads
    renewed = jnp.exp(cumul[..., -1])[..., None, None] * saved + jnp.einsum(
        "bhpk,bhpv->bhkv", tail, update, precision=highest
    )
    return (jnp.transpose(output, (0, 2, 1, 3)), renewed)


def body(
    tokens,
    in_gain,
    w_query,
    w_key,
    w_value,
    w_gate,
    w_beta,
    w_decay,
    decay_base,
    out_gain,
    w_out,
    state,
    prev_keys,
    prev_values,
    prev_beta,
    prev_decay,
    accepted,
):
    seq_count, props, _ = tokens.shape
    heads = decay_base.shape[0]
    head_size = out_gain.shape[0]
    width = heads * head_size
    rows = seq_count * props
    whole = lax.all_gather(tokens, "tp", axis=2, tiled=True)
    wide = whole.astype(jnp.float32)
    normed = (wide * lax.rsqrt(jnp.mean(wide * wide, -1, keepdims=True) + EPS) * in_gain).astype(
        jnp.bfloat16
    )
    normed = normed.reshape(rows, -1)

    def add_rows(piece):
        return jnp.dot(normed, piece, preferred_element_type=jnp.float32)

    query = add_rows(lax.all_gather(w_query, "kv", axis=0, tiled=True))
    key_vec = add_rows(lax.all_gather(w_key, "kv", axis=0, tiled=True))
    value_vec = add_rows(lax.all_gather(w_value, "kv", axis=0, tiled=True))
    gate = add_rows(lax.all_gather(w_gate, "kv", axis=0, tiled=True))
    offset = lax.axis_index("tp") * heads
    beta_cols = lax.dynamic_slice_in_dim(w_beta, offset, heads, 1)
    decay_cols = lax.dynamic_slice_in_dim(w_decay, offset, heads, 1)
    shape4 = (seq_count, props, heads, head_size)
    query = normalize_rows(query.reshape(shape4)) * head_size ** (-0.5)
    key_vec = normalize_rows(key_vec.reshape(shape4))
    value_vec = value_vec.reshape(shape4)
    gate = gate.reshape(shape4)
    strength = jax.nn.sigmoid(
        jnp.dot(normed, beta_cols, preferred_element_type=jnp.float32)
    ).reshape(seq_count, props, heads)
    log_decay = (
        -decay_base
        * jax.nn.softplus(jnp.dot(normed, decay_cols, preferred_element_type=jnp.float32))
    ).reshape(seq_count, props, heads)
    live = (jnp.arange(props, dtype=jnp.int32)[None, :] < accepted[:, None]).astype(jnp.float32)
    prev_strength = jax.nn.sigmoid(prev_beta) * live[..., None]
    prev_log = prev_decay * live[..., None]
    prev_k = normalize_rows(prev_keys.astype(jnp.float32).reshape(shape4))
    prev_v = prev_values.astype(jnp.float32).reshape(shape4)
    saved = jnp.transpose(state.reshape(seq_count, head_size, heads, head_size), (0, 2, 1, 3))
    committed = delta_block(saved, prev_k, prev_k, prev_v, prev_strength, prev_log)[1]
    output = delta_block(committed, query, key_vec, value_vec, strength, log_decay)[0]
    gated = (
        (
            output
            * lax.rsqrt(jnp.mean(output * output, -1, keepdims=True) + EPS)
            * out_gain
            * jax.nn.silu(gate)
        )
        .astype(jnp.bfloat16)
        .reshape(rows, width)
    )
    new_state = jnp.transpose(committed, (0, 2, 1, 3)).reshape(seq_count, head_size, width)
    terms = jnp.dot(
        gated, lax.all_gather(w_out, "kv", axis=1, tiled=True), preferred_element_type=jnp.float32
    )
    mixed = lax.psum_scatter(terms.astype(jnp.bfloat16), "tp", scatter_dimension=1, tiled=True)
    return (mixed.reshape(seq_count, props, -1), new_state)


def solution(mesh):
    placed = (
        P(("grp", "kv"), None, "tp"),
        P(),
        P("kv", "tp"),
        P("kv", "tp"),
        P("kv", "tp"),
        P("kv", "tp"),
        P(),
        P(),
        P("tp"),
        P(),
        P("tp", "kv"),
        P(("grp", "kv"), None, "tp"),
        P(("grp", "kv"), None, "tp"),
        P(("grp", "kv"), None, "tp"),
        P(("grp", "kv"), None, "tp"),
        P(("grp", "kv"), None, "tp"),
        P(("grp", "kv")),
    )
    return jax.shard_map(
        body,
        mesh=mesh,
        in_specs=placed,
        out_specs=(P(("grp", "kv"), None, "tp"), P(("grp", "kv"), None, "tp")),
        check_vma=False,
    )
```

profile of v0, /device:TPU:0, one launch (start us, length us, event | category | flops | bytes accessed | tf_op | source)
XLA Modules:
  0.0 192.2 jit_solution(15288922309329087683)
XLA Ops:
  10.6 8.9 %all_gather.18 = bf16[32,4,2048]{2,1,0:T(4,128)(2,1)S(1)} all-gather(bf16[32,4,512]{2,1,0:T(4,128)(2,1)} %param.17), channel_id=1, replica_groups=mesh['grp'=2,'kv'=4,'tp'=4] {'tp'}, dimensions={2}, use_global_device_ids=true | all-gather | bytes 655360 | tf_op jit(solution)/shard_map/all_gather | solution.py:82
  19.9 1.8 fusion.93
  27.6 3.3 %reshape.139 = f32[32,64,4,64]{3,2,1,0:T(4,128)} reshape(f32[32,64,256]{2,1,0:T(8,128)S(1)} %copy-done.4) | data formatting | bytes 4194304 | tf_op jit(solution)/shard_map/reshape | solution.py:116
  32.2 1.4 fusion.12
  36.0 1.5 multiply_subtract_fusion
  37.8 5.7 %fusion.8 = f32[32,4,4,64]{3,2,1,0:T(4,128)S(1)} fusion(f32[32,64,4,64]{3,2,1,0:T(4,128)} %reshape.139, f32[32,4,4,128]{3,2,1,0:T(4,128)S(1)} %pad_maximum_fusion), kind=kOutput, calls=%fused_computation.11 | convolution fusion | flops 25198592 | bytes 2752512 | tf_op jit(solution)/shard_map/bhpk,bhkv->bhpv/dot_general | solution.py:44
  43.5 9.6 %bitcast_add_fusion = (f32[32,64,4,64]{3,1,2,0:T(8,128)}, f32[32,4,64,64]{3,2,1,0:T(8,128)}) fusion(f32[32,64,4,64]{3,2,1,0:T(4,128)S(1)} %copy-done.1, f32[32,4]{1,0:T(8,128)S(1)} %copy.381, f32[32,4,4,64]{3,2,1,0:T(4,128)S(1)} %fusion.8, f32[32,4,4,64]{3,2,0,1:T(4,128)S(1)} %reshape.148, f32[32,4,4]{1,2,0:T(4,128)S(1)} %copy.387, f32[32,4,4]{2,1,0:T(4,128)S(1)} %copy.383), kind=kOutput, calls=%fused_computation | convolution fusion | flops 26279936 | bytes 6558208 | tf_op jit(solution)/shard_map/bhpk,bhpv->bhkv/dot_general | solution.py:52
  53.1 1.5 copy.436
  54.7 14.6 %all-gather.6.cloned.1.call-done = bf16[2048,256]{1,0:T(8,128)(2,1)} async-done(((bf16[512,256]{1,0:T(8,128)(2,1)}), bf16[2048,256]{1,0:T(8,128)(2,1)}) %all-gather.6.cloned.1.call-update) | async-done | bytes 1048592 | tf_op jit(solution)/shard_map/all_gather | solution.py:92
  69.3 1.5 copy.377
  72.2 26.0 %all-gather.8.cloned.1.call-done = bf16[2048,256]{1,0:T(8,128)(2,1)} async-done(((bf16[512,256]{1,0:T(8,128)(2,1)}), bf16[2048,256]{1,0:T(8,128)(2,1)}) %all-gather.8.cloned.1.call-update) | async-done | bytes 1048592 | tf_op jit(solution)/shard_map/all_gather | solution.py:93
  98.3 1.7 copy.409
  100.0 1.4 multiply_reduce_fusion
  102.0 25.1 %all-gather.10.cloned.1.call-done = bf16[2048,256]{1,0:T(8,128)(2,1)} async-done(((bf16[512,256]{1,0:T(8,128)(2,1)}), bf16[2048,256]{1,0:T(8,128)(2,1)}) %all-gather.10.cloned.1.call-update) | async-done | bytes 1048592 | tf_op jit(solution)/shard_map/all_gather | solution.py:94
  127.1 1.5 copy.417
  128.6 1.3 fusion.42
  129.9 2.0 %convolution_multiply_fusion.1 = f32[32,4,4,4]{3,2,1,0:T(4,128)S(1)} fusion(f32[32,4,4,64]{3,0,1,2:T(8,128)S(1)} %get-tuple-element.15, f32[32,4,4,64]{3,0,1,2:T(8,128)S(1)} %get-tuple-element.38, f32[32,4,4]{2,1,0:T(4,128)S(1)} %copy.413, pred[4,4]{1,0:T(4,128)(4,1)} %copy-done.13), kind=kOutput, calls=%fused_computation.14 | convolution fusion | flops 1581056 | bytes 272400 | tf_op jit(solution)/shard_map/bhik,bhjk->bhij/dot_general | solution.py:47
  131.9 2.0 %fusion.11 = f32[32,4,4,4]{3,2,1,0:T(4,128)S(1)} fusion(f32[32,4,4,64]{3,0,1,2:T(8,128)S(1)} %get-tuple-element.38, f32[32,4,4]{2,1,0:T(4,128)} %bitcast.126, f32[32,4,4]{2,1,0:T(4,128)S(1)} %copy.413, pred[4,4]{1,0:T(4,128)(4,1)} %copy-done.13, pred[4,4]{1,0:T(4,128)(4,1)} %copy-done.14), kind=kOutput, calls=%fused_computation.13 | convolution fusion | flops 1585152 | bytes 143392 | tf_op jit(solution)/shard_map/bhik,bhjk->bhij/dot_general | solution.py:29
  133.9 1.2 fusion.82
  135.1 1.5 copy.428
  136.6 1.5 copy.427
  138.1 1.5 copy.426
  139.6 1.5 copy.425
  141.1 1.5 copy.424
  143.2 1.4 fusion.13
  145.8 8.0 %fusion.4 = f32[32,4,4,64]{3,2,1,0:T(4,128)S(1)} fusion(f32[32,4,64,64]{3,2,1,0:T(8,128)} %get-tuple-element.36, f32[32,64,4,64]{3,2,1,0:T(4,128)} %reshape.139, f32[32,4]{1,0:T(8,128)S(1)} %copy.381, f32[32,4,4,64]{3,0,1,2:T(8,128)S(1)} %slice.129), kind=kOutput, calls=%fused_computation.7 | convolution fusion | flops 26214400 | bytes 4456960 | tf_op jit(solution)/shard_map/bhpk,bhkv->bhpv/dot_general | solution.py:44
  155.1 3.8 %fusion.6 = f32[32,4,4,64]{3,2,1,0:T(4,128)S(1)} fusion(f32[32,4,64,64]{3,2,1,0:T(8,128)S(1)} %copy-done.3, f32[32,64,4,64]{3,2,1,0:T(4,128)S(1)} %copy-done.2, f32[32,4]{1,0:T(8,128)S(1)} %copy.381, f32[32,4,4,64]{3,0,1,2:T(8,128)S(1)} %get-tuple-element.14), kind=kOutput, calls=%fused_computation.8 | convolution fusion | flops 26214400 | bytes 4456960 | tf_op jit(solution)/shard_map/bhpk,bhkv->bhpv/dot_general | solution.py:48
  160.2 2.4 %convolution_convert_fusion = bf16[128,2048]{1,0:T(8,128)(2,1)} fusion(bf16[128,256]{1,0:T(8,128)(2,1)S(1)} %reshape.144, bf16[256,2048]{1,0:T(8,128)(2,1)} %all-gather.14.cloned.1.call-done), kind=kOutput, calls=%fused_computation.6 | convolution fusion | flops 134479872 | bytes 1638400 | tf_op jit(solution)/shard_map/dot_general | solution.py:130
  162.6 7.8 %copy.441 = f32[32,64,4,64]{3,2,1,0:T(4,128)} copy(f32[32,64,4,64]{3,1,2,0:T(8,128)} %get-tuple-element.35) | data formatting | bytes 4194304 | tf_op jit(solution)/shard_map/add | solution.py:52
  170.3 5.3 %reshape.146 = f32[32,64,256]{2,1,0:T(8,128)} reshape(f32[32,64,4,64]{3,2,1,0:T(4,128)} %copy.441) | data formatting | bytes 4194304 | tf_op jit(solution)/shard_map/reshape | solution.py:129
  175.6 8.1 %reduce-scatter.2.cloned.1.call-done = bf16[128,512]{1,0:T(8,128)(2,1)} async-done(((bf16[128,2048]{1,0:T(8,128)(2,1)}), bf16[128,512]{1,0:T(8,128)(2,1)}) %reduce-scatter.2.cloned.1.call-update) | async-done | bytes 131088 | tf_op jit(solution)/shard_map/reduce_scatter | solution.py:133
  183.8 1.6 reshape.145
  (108 shorter events, 19.6 us)
Async XLA Ops:
  7.2 15.8 %copy-start = (bf16[2048,16]{0,1:T(8,128)(2,1)S(1)}, bf16[2048,16]{0,1:T(8,128)(2,1)}, u32[]{:S(2)}) copy-start(bf16[2048,16]{0,1:T(8,128)(2,1)} %param.23) | copy-start | bytes 196612
  7.2 17.6 %copy-start.10 = (s32[32]{0:T(128)S(1)}, s32[32]{0:T(128)}, u32[]{:S(2)}) copy-start(s32[32]{0:T(128)} %param.33) | copy-start | bytes 388
  7.2 17.6 %copy-start.8 = (f32[32,4,4]{0,2,1:T(4,128)S(1)}, f32[32,4,4]{0,2,1:T(4,128)}, u32[]{:S(2)}) copy-start(f32[32,4,4]{0,2,1:T(4,128)} %param.32) | copy-start | bytes 6148
  7.2 17.8 %copy-start.11 = (f32[4]{0:T(128)S(1)}, f32[4]{0:T(128)}, u32[]{:S(2)}) copy-start(f32[4]{0:T(128)} %param.25) | copy-start | bytes 52
  7.2 20.4 %copy-start.4 = (f32[32,64,256]{2,1,0:T(8,128)S(1)}, f32[32,64,256]{2,1,0:T(8,128)}, u32[]{:S(2)}) copy-start(f32[32,64,256]{2,1,0:T(8,128)} %param.28) | copy-start | bytes 6291460
  7.2 45.9 %all-gather.12.cloned.1.call-start = ((), (), s32[]{:S(2)}) async-start(), calls=%async_computation.4 | async-start | bytes 1310720 | tf_op jit(solution)/shard_map/all_gather | solution.py:95
  8.0 61.3 %all-gather.6.cloned.1.call-start = ((), (), s32[]{:S(2)}) async-start(), calls=%async_computation.1 | async-start | bytes 1310720 | tf_op jit(solution)/shard_map/all_gather | solution.py:92
  8.7 89.6 %all-gather.8.cloned.1.call-start = ((), (), s32[]{:S(2)}) async-start(), calls=%async_computation.2 | async-start | bytes 1310720 | tf_op jit(solution)/shard_map/all_gather | solution.py:93
  9.4 117.6 %all-gather.10.cloned.1.call-start = ((), (), s32[]{:S(2)}) async-start(), calls=%async_computation.3 | async-start | bytes 1310720 | tf_op jit(solution)/shard_map/all_gather | solution.py:94
  10.0 150.1 %all-gather.14.cloned.1.call-start = ((), (), s32[]{:S(2)}) async-start(), calls=%async_computation.5 | async-start | bytes 1310720 | tf_op jit(solution)/shard_map/all_gather | solution.py:131
  10.6 173.2 %reduce-scatter.2.cloned.1.call-start = ((), (), s32[]{:S(2)}) async-start(), calls=%async_computation.6 | async-start | bytes 655360 | tf_op jit(solution)/shard_map/reduce_scatter | solution.py:133
  22.8 9.4 %copy-start.13 = (pred[4,4]{1,0:T(4,128)(4,1)}, pred[4,4]{1,0:T(4,128)(4,1)S(1)}, u32[]{:S(2)}) copy-start(pred[4,4]{1,0:T(4,128)(4,1)S(1)} %get-tuple-element.39) | copy-start | bytes 52
  22.8 9.4 %copy-start.14 = (pred[4,4]{1,0:T(4,128)(4,1)}, pred[4,4]{1,0:T(4,128)(4,1)S(1)}, u32[]{:S(2)}) copy-start(pred[4,4]{1,0:T(4,128)(4,1)S(1)} %get-tuple-element.40) | copy-start | bytes 52
  22.9 8.1 %copy-start.6 = (bf16[32,4,256]{2,1,0:T(4,128)(2,1)S(1)}, bf16[32,4,256]{2,1,0:T(4,128)(2,1)}, u32[]{:S(2)}) copy-start(bf16[32,4,256]{2,1,0:T(4,128)(2,1)} %param.30) | copy-start | bytes 196612
  22.9 8.3 %copy-start.9 = (f32[32,4,4]{0,2,1:T(4,128)S(1)}, f32[32,4,4]{0,2,1:T(4,128)}, u32[]{:S(2)}) copy-start(f32[32,4,4]{0,2,1:T(4,128)} %param.31) | copy-start | bytes 6148
  22.9 8.4 %copy-start.7 = (bf16[32,4,256]{2,1,0:T(4,128)(2,1)S(1)}, bf16[32,4,256]{2,1,0:T(4,128)(2,1)}, u32[]{:S(2)}) copy-start(bf16[32,4,256]{2,1,0:T(4,128)(2,1)} %param.29) | copy-start | bytes 196612
  35.5 8.0 %copy-start.1 = (f32[32,64,4,64]{3,2,1,0:T(4,128)S(1)}, f32[32,64,4,64]{3,2,1,0:T(4,128)}, u32[]{:S(2)}) copy-start(f32[32,64,4,64]{3,2,1,0:T(4,128)} %reshape.139) | copy-start | bytes 6291460
  53.1 17.7 %copy-start.5 = (bf16[32,4,2048,1]{2,1,0,3:T(4,128)(2,1)S(1)}, bf16[32,4,2048,1]{2,1,0,3:T(4,128)(2,1)}, u32[]{:S(2)}) copy-start(bf16[32,4,2048,1]{2,1,0,3:T(4,128)(2,1)} %fusion.93) | copy-start | bytes 1572868
  145.8 9.3 %copy-start.2 = (f32[32,64,4,64]{3,2,1,0:T(4,128)S(1)}, f32[32,64,4,64]{3,2,1,0:T(4,128)}, u32[]{:S(2)}) copy-start(f32[32,64,4,64]{3,2,1,0:T(4,128)} %reshape.139) | copy-start | bytes 6291460
  145.8 9.3 %copy-start.3 = (f32[32,4,64,64]{3,2,1,0:T(8,128)S(1)}, f32[32,4,64,64]{3,2,1,0:T(8,128)}, u32[]{:S(2)}) copy-start(f32[32,4,64,64]{3,2,1,0:T(8,128)} %get-tuple-element.36) | copy-start | bytes 6291460
  155.1 4.0 %copy-start.12 = (f32[64]{0:T(128)S(1)}, f32[64]{0:T(128)}, u32[]{:S(2)}) copy-start(f32[64]{0:T(128)} %param.26) | copy-start | bytes 772
Sparse Core Ops, SparseCore 0:
  9.6 30.6 all-gather.11
  41.9 27.3 all-gather.5
  70.9 27.3 all-gather.7
  99.7 27.3 all-gather.9
  128.5 27.3 all-gather.13
  162.7 21.0 reduce-scatter.1
where the time goes:
time: 193 us; the launch traced here: 192 us
  waiting for transfers between devices  77.1 us (40%)
  matrix products  41.6 us (22%)
  local copies, waits for them, and re-layouts  40.1 us (21%)
  between operations  14.6 us (8%)
  other arithmetic  9.67 us (5%)
  blocking collectives  8.86 us (5%)
    all_gather x1, waiting for transfers between devices, body(): key_vec = add_rows(lax.all_gather(w_key, 'kv', axis=0, tiled=True))  26 us
    all_gather x1, waiting for transfers between devices, body(): value_vec = add_rows(lax.all_gather(w_value, 'kv', axis=0, tiled=True))  25.1 us
    all_gather x1, waiting for transfers between devices, body(): query = add_rows(lax.all_gather(w_query, 'kv', axis=0, tiled=True))  14.6 us
    dot_general x2, matrix products, delta_block(): jnp.einsum('bhpk,bhkv->bhpv', solution[..., value_size:], saved, precisio...  13.7 us
    slice x14, local copies, waits for them, and re-layouts, delta_block(): lower_mat[:, :, row_index, col_index, None] * solved[col_index]  10.5 us
    dot_general x1, matrix products, delta_block(): jnp.einsum('bhpk,bhpv->bhkv', tail, update, precision=highest)  9.64 us
    all_gather x1, blocking collectives, body(): whole = lax.all_gather(tokens, 'tp', axis=2, tiled=True)  8.86 us
    reduce_scatter x1, waiting for transfers between devices, body(): lax.psum_scatter(terms.astype(jnp.bfloat16), 'tp', scatter_dimension=1, t...  8.14 us
  transfers between devices with their start and end apart: 6, of which 4 were waited for; matrix products, arithmetic and copies ran while one was open for 45% of the time, Pallas kernels for 0%

commit v1 on v0

v1 whole, which is shorter than its diff:
```python
import functools

import jax
import jax.numpy as jnp
from jax import lax
from jax.experimental import pallas as pl
from jax.experimental.pallas import tpu as pltpu
from jax.sharding import PartitionSpec as P

EPS = 1e-06
F32 = jnp.float32
BF16 = jnp.bfloat16
MESH = pl.DeviceIdType.MESH


def kernel(
    cfg,
    tok_hbm, gain_ref, wq_hbm, wk_hbm, wv_hbm, wg_hbm, wb_ref, wd_ref, base_ref, og_ref, wo_hbm,
    state_hbm, pk_ref, pv_ref, pb_ref, pd_ref, acc_ref,
    mixed_ref, new_hbm,
    tok, wp, wo, st, normed, kq, res, tk, up, al, rows_a, rows_b, proj, send_buf, recv_buf,
    in_sem, own_sem, zr_send, zl_send, z_recv, y_send, y_recv, t_send, t_recv, r_send, r_recv,
    out_sem,
):
    n_grp, n_kv, n_tp, seqs, props, heads, hd, gather_out = cfg
    width = heads * hd
    g = lax.axis_index("grp")
    k = lax.axis_index("kv")
    t_me = lax.axis_index("tp")
    rows = seqs * props
    own_rows = wk_hbm.shape[0]
    piece = own_rows // n_grp
    out_piece = wo.shape[1] // n_grp
    sources = [wk_hbm, wq_hbm, wv_hbm, wg_hbm]
    n_mat = len(sources) + (1 if gather_out else 0)

    tok_in = pltpu.make_async_copy(tok_hbm, tok.at[t_me], in_sem.at[0])
    tok_in.start()
    own_copies = []
    for m in range(n_mat):
        if m < len(sources):
            dst = wp.at[m, pl.ds(k * own_rows, own_rows), :]
            copy = pltpu.make_async_copy(sources[m], dst, own_sem.at[m])
        else:
            copy = pltpu.make_async_copy(wo_hbm, wo.at[k], own_sem.at[m])
        copy.start()
        own_copies.append(copy)
    state_in = pltpu.make_async_copy(state_hbm, st, in_sem.at[1])
    state_in.start()
    out_in = None
    if not gather_out:
        out_in = pltpu.make_async_copy(wo_hbm, wo, own_sem.at[n_mat])
        out_in.start()

    barrier = pltpu.get_barrier_semaphore()

    def greet(dev):
        pl.semaphore_signal(barrier, inc=1, device_id=dev, device_id_type=MESH)

    @pl.when(k > 0)
    def _():
        greet({"kv": k - 1})

    @pl.when(k < n_kv - 1)
    def _():
        greet({"kv": k + 1})

    for d in range(1, n_grp):
        greet({"grp": lax.rem(g + d, n_grp)})
    for d in range(1, n_tp):
        greet({"tp": lax.rem(t_me + d, n_tp)})

    beside = jnp.minimum(k, 1) + jnp.minimum(n_kv - 1 - k, 1)
    pl.semaphore_wait(barrier, n_grp + n_tp - 2 + beside)

    def slot(m, origin, part):
        if m < len(sources):
            return wp.at[m, pl.ds(origin * own_rows + part * piece, piece), :]
        return wo.at[origin, pl.ds(part * out_piece, out_piece), :]

    def z_right(m, origin):
        ref = slot(m, origin, g)
        return pltpu.make_async_remote_copy(
            ref, ref, zr_send.at[m, origin], z_recv.at[m, origin],
            device_id={"kv": k + 1}, device_id_type=MESH)

    def z_left(m, origin):
        ref = slot(m, origin, g)
        return pltpu.make_async_remote_copy(
            ref, ref, zl_send.at[m, origin], z_recv.at[m, origin],
            device_id={"kv": k - 1}, device_id_type=MESH)

    def y_copy(m, origin, d):
        ref = slot(m, origin, g)
        return pltpu.make_async_remote_copy(
            ref, ref, y_send.at[d - 1, m, origin], y_recv.at[d - 1, m, origin],
            device_id={"grp": lax.rem(g + d, n_grp)}, device_id_type=MESH)

    def y_wait(m, origin, d):
        ref = slot(m, origin, lax.rem(g + n_grp - d, n_grp))
        pltpu.make_async_remote_copy(
            ref, ref, y_send.at[d - 1, m, origin], y_recv.at[d - 1, m, origin],
            device_id={"grp": lax.rem(g + d, n_grp)}, device_id_type=MESH).wait_recv()

    def send_own(m):
        own_copies[m].wait()

        @pl.when(k < n_kv - 1)
        def _():
            z_right(m, k).start()

        @pl.when(k > 0)
        def _():
            z_left(m, k).start()

    def forward(m):
        def step(s, carry):
            left = k - 1 - s
            right = k + 1 + s

            @pl.when(left >= 0)
            def _():
                z_right(m, left).wait_recv()

                @pl.when(k < n_kv - 1)
                def _():
                    z_right(m, left).start()

                for d in range(1, n_grp):
                    y_copy(m, left, d).start()

            @pl.when(right < n_kv)
            def _():
                z_left(m, right).wait_recv()

                @pl.when(k > 0)
                def _():
                    z_left(m, right).start()

                for d in range(1, n_grp):
                    y_copy(m, right, d).start()

            return carry

        lax.fori_loop(0, n_kv - 1, step, 0)

    def wait_y(m):
        def step(o, carry):
            @pl.when(o != k)
            def _():
                for d in range(1, n_grp):
                    y_wait(m, o, d)

            return carry

        lax.fori_loop(0, n_kv, step, 0)

    def t_copy(d):
        return pltpu.make_async_remote_copy(
            tok.at[t_me], tok.at[t_me], t_send.at[d - 1], t_recv.at[d - 1],
            device_id={"tp": lax.rem(t_me + d, n_tp)}, device_id_type=MESH)

    def t_wait(d):
        origin = lax.rem(t_me + n_tp - d, n_tp)
        pltpu.make_async_remote_copy(
            tok.at[origin], tok.at[origin], t_send.at[d - 1], t_recv.at[d - 1],
            device_id={"tp": lax.rem(t_me + d, n_tp)}, device_id_type=MESH).wait_recv()

    send_own(0)
    tok_in.wait()
    for d in range(1, n_tp):
        t_copy(d).start()
    send_own(1)

    blk = (
        lax.broadcasted_iota(jnp.int32, (width, width), 0) // hd
        == lax.broadcasted_iota(jnp.int32, (width, width), 1) // hd
    ).astype(F32).astype(BF16)
    lane_head = lax.broadcasted_iota(jnp.int32, (1, width), 1) // hd
    masks = [(lane_head == h).astype(F32) for h in range(heads)]

    def head_sum(x):
        hi = x.astype(BF16)
        lo = (x - hi.astype(F32)).astype(BF16)
        return jnp.dot(hi, blk, preferred_element_type=F32) + jnp.dot(
            lo, blk, preferred_element_type=F32)

    lanes = 128
    blocks = width // lanes

    def rd(ref, at, *lead):
        return jnp.concatenate([ref[(*lead, c, at)] for c in range(blocks)], axis=-1)

    def wr(ref, at, x, *lead):
        for c in range(blocks):
            ref[(*lead, c, at)] = x[:, c * lanes : (c + 1) * lanes]

    every = pl.ds(0, rows)

    def spread(x):
        total = jnp.zeros((x.shape[0], width), F32)
        for h in range(heads):
            total = jnp.where(lane_head == h, x[:, h : h + 1], total)
        return total

    pad = 2 * props

    def by_state(s, carry):
        tile = st[pl.ds(pl.multiple_of(s * hd, hd), hd), :]
        stacked = jnp.concatenate([(tile * mask).astype(BF16) for mask in masks], axis=0)
        at = pl.ds(pl.multiple_of(s * pad, pad), pad)
        lhs = rd(kq, at).astype(BF16)
        wr(res, at, jnp.dot(lhs, stacked, preferred_element_type=F32))
        return carry

    def solve(keys, values, weights, logs, queries):
        cumul = []
        run = None
        for t in range(props):
            run = logs[t] if run is None else run + logs[t]
            cumul.append(run)
        low = [(i, j) for i in range(props) for j in range(i)]
        products = [keys[i] * keys[j] for i, j in low]
        full = []
        if queries is not None:
            full = [(i, j) for i in range(props) for j in range(i + 1)]
            products += [queries[i] * keys[j] for i, j in full]
        sums = head_sum(jnp.concatenate(products, axis=0))
        sums = [sums[i * seqs : (i + 1) * seqs] for i in range(len(products))]
        kk = dict(zip(low, sums))
        qk = dict(zip(full, sums[len(low):]))
        dec = {pair: jnp.exp(cumul[pair[0]] - cumul[pair[1]]) for pair in low}
        growth = [jnp.exp(c) for c in cumul]
        update = []
        for t in range(props):
            seen = rd(res, pl.ds(t, seqs, stride=pad))
            term = values[t] - growth[t] * seen
            for j in range(t):
                term = term - kk[t, j] * dec[t, j] * update[j]
            update.append(weights[t] * term)
        outs = []
        if queries is not None:
            for t in range(props):
                out = growth[t] * rd(res, pl.ds(props + t, seqs, stride=pad))
                for j in range(t + 1):
                    score = qk[t, j] if j == t else qk[t, j] * dec[t, j]
                    out = out + score * update[j]
                outs.append(out)
        return cumul, growth, update, outs

    def split(ref):
        return [rd(ref, pl.ds(t, seqs, stride=props)) for t in range(props)]

    pk = pk_ref[...].astype(F32)
    wr(rows_a, every, pk * lax.rsqrt(head_sum(pk * pk) + EPS))
    wr(rows_b, every, pv_ref[...].astype(F32))
    keys = split(rows_a)
    values = split(rows_b)
    accepted = jnp.broadcast_to(acc_ref[...], (seqs, width))
    weights, logs = [], []
    for t in range(props):
        live = (accepted > t).astype(F32)
        weights.append(spread(jax.nn.sigmoid(pb_ref[:, t, :])) * live)
        logs.append(spread(pd_ref[:, t, :]) * live)
        wr(kq, pl.ds(t, seqs, stride=pad), keys[t])
        wr(kq, pl.ds(props + t, seqs, stride=pad), keys[t])
    state_in.wait()
    lax.fori_loop(0, seqs, by_state, 0, unroll=4)
    cumul, growth, update, _ = solve(keys, values, weights, logs, None)
    al[...] = growth[-1]
    for t in range(props):
        wr(tk, pl.ds(t, seqs, stride=pad), jnp.exp(cumul[-1] - cumul[t]) * keys[t])
        wr(up, pl.ds(t, seqs, stride=pad), update[t])
        wr(tk, pl.ds(props + t, seqs, stride=pad), jnp.zeros((seqs, width), F32))
        wr(up, pl.ds(props + t, seqs, stride=pad), jnp.zeros((seqs, width), F32))

    def renew(s, carry):
        at = pl.ds(pl.multiple_of(s * pad, pad), pad)
        outer = lax.dot_general(
            rd(tk, at), rd(up, at), (((0,), (0,)), ((), ())), preferred_element_type=F32)
        where = pl.ds(pl.multiple_of(s * hd, hd), hd)
        tile = al[pl.ds(s, 1), :] * st[where, :]
        for h in range(heads):
            tile = tile + masks[h] * outer[h * hd : (h + 1) * hd, :]
        st[where, :] = tile
        return carry

    lax.fori_loop(0, seqs, renew, 0, unroll=2)
    state_out = pltpu.make_async_copy(st, new_hbm, out_sem)
    state_out.start()

    for d in range(1, n_tp):
        t_wait(d)
    square = jnp.zeros((rows, 1), F32)
    for i in range(n_tp):
        wide = tok[i].astype(F32)
        square = square + jnp.sum(wide * wide, -1, keepdims=True)
    feats = tok.shape[2]
    scale = lax.rsqrt(square / (n_tp * feats) + EPS)
    for i in range(n_tp):
        cols = slice(i * feats, (i + 1) * feats)
        normed[:, cols] = (tok[i].astype(F32) * scale * gain_ref[:, cols]).astype(BF16)
    all_heads = wb_ref.shape[1]
    pick = (
        lax.broadcasted_iota(jnp.int32, (all_heads, width), 0)
        == t_me * heads + lax.broadcasted_iota(jnp.int32, (all_heads, width), 1) // hd
    ).astype(F32)

    def per_head(ref):
        raw = jnp.dot(normed[...], ref[...], preferred_element_type=F32)
        return jnp.dot(raw, pick, precision=lax.Precision.HIGHEST, preferred_element_type=F32)

    wr(rows_a, every, jax.nn.sigmoid(per_head(wb_ref)))
    weights = split(rows_a)
    base = jnp.zeros((1, width), F32)
    for h in range(heads):
        base = jnp.where(lane_head == h, base_ref[h], base)
    wr(rows_b, every, -base * jax.nn.softplus(per_head(wd_ref)))
    logs = split(rows_b)

    def project(m):
        return jnp.dot(normed[...], wp[m], preferred_element_type=F32)

    def finish(m):
        wait_y(m)
        if m < len(sources):
            value = project(m)
            if m == 0:
                value = value * lax.rsqrt(head_sum(value * value) + EPS)
            elif m == 1:
                value = value * lax.rsqrt(head_sum(value * value) + EPS) * hd ** (-0.5)
            wr(proj, every, value, m)

    outs = None
    for m in range(n_mat):
        if m >= 1 and m + 1 < n_mat:
            send_own(m + 1)
        forward(m)
        if m >= 1:
            finish(m - 1)
        if m == 3:
            keys = [rd(proj, pl.ds(t, seqs, stride=props), 0) for t in range(props)]
            queries = [rd(proj, pl.ds(t, seqs, stride=props), 1) for t in range(props)]
            values = [rd(proj, pl.ds(t, seqs, stride=props), 2) for t in range(props)]
            for t in range(props):
                wr(kq, pl.ds(t, seqs, stride=pad), keys[t])
                wr(kq, pl.ds(props + t, seqs, stride=pad), queries[t])
            lax.fori_loop(0, seqs, by_state, 0, unroll=4)
            outs = solve(keys, values, weights, logs, queries)[3]
            for t in range(props):
                wr(rows_a, pl.ds(t, seqs, stride=props), outs[t])
            out = rd(rows_a, every)
            out = out * lax.rsqrt(head_sum(out * out) / hd + EPS)
            tile_gain = (
                lax.broadcasted_iota(jnp.int32, (hd, width), 0)
                == lax.broadcasted_iota(jnp.int32, (hd, width), 1) % hd
            ).astype(F32)
            gain = jnp.dot(
                jnp.broadcast_to(og_ref[...], (8, hd)), tile_gain,
                precision=lax.Precision.HIGHEST, preferred_element_type=F32)[:1]
            wr(rows_a, every, out * gain)
    if not gather_out:
        finish(n_mat - 1)
        out_in.wait()
    gate = rd(proj, every, 3)
    gated = (rd(rows_a, every) * (gate / (1.0 + jnp.exp(-gate)))).astype(BF16)
    if gather_out:
        finish(n_mat - 1)

    def r_copy(d):
        dest = lax.rem(t_me + d, n_tp)
        return pltpu.make_async_remote_copy(
            send_buf.at[d - 1], recv_buf.at[d - 1], r_send.at[d - 1], r_recv.at[d - 1],
            device_id={"tp": dest}, device_id_type=MESH)

    order = sorted(range(1, n_tp), key=lambda d: -min(d, n_tp - d))
    for d in order:
        dest = lax.rem(t_me + d, n_tp)
        send_buf[d - 1] = jnp.dot(gated, wo[dest], preferred_element_type=F32).astype(BF16)
        r_copy(d).start()
    total = jnp.dot(gated, wo[t_me], preferred_element_type=F32)
    for d in reversed(order):
        r_copy(d).wait_recv()
        total = total + recv_buf[d - 1].astype(F32)
    mixed_ref[...] = total.astype(BF16)

    for d in range(1, n_tp):
        t_copy(d).wait_send()
        r_copy(d).wait_send()

    def drain(m):
        def step(o, carry):
            @pl.when(jnp.logical_and(o <= k, k < n_kv - 1))
            def _():
                z_right(m, o).wait_send()

            @pl.when(jnp.logical_and(o >= k, k > 0))
            def _():
                z_left(m, o).wait_send()

            @pl.when(o != k)
            def _():
                for d in range(1, n_grp):
                    y_copy(m, o, d).wait_send()

            return carry

        lax.fori_loop(0, n_kv, step, 0)

    for m in range(n_mat):
        drain(m)
    state_out.wait()


def body(
    sizes,
    tokens, in_gain, w_query, w_key, w_value, w_gate, w_beta, w_decay, decay_base, out_gain, w_out,
    state, prev_keys, prev_values, prev_beta, prev_decay, accepted,
):
    n_grp, n_kv, n_tp = sizes
    seqs, props, feats = tokens.shape
    heads = decay_base.shape[0]
    hd = out_gain.shape[0]
    width = heads * hd
    rows = seqs * props
    pad = 2 * props
    gather_out = n_kv == n_tp
    if not gather_out:
        w_out = lax.all_gather(w_out, "kv", axis=1, tiled=True)
        w_out = jnp.transpose(w_out.reshape(width, n_tp, feats), (1, 0, 2))
    n_mat = 5 if gather_out else 4
    cfg = (n_grp, n_kv, n_tp, seqs, props, heads, hd, gather_out)
    vmem = pl.BlockSpec(memory_space=pltpu.VMEM)
    hbm = pl.BlockSpec(memory_space=pl.ANY)
    smem = pl.BlockSpec(memory_space=pltpu.SMEM)
    dma = pltpu.SemaphoreType.DMA
    mixed, new_state = pl.pallas_call(
        functools.partial(kernel, cfg),
        out_shape=(
            jax.ShapeDtypeStruct((rows, feats), BF16),
            jax.ShapeDtypeStruct((seqs * hd, width), F32),
        ),
        in_specs=[hbm, vmem, hbm, hbm, hbm, hbm, vmem, vmem, smem, vmem, hbm, hbm,
                  vmem, vmem, vmem, vmem, vmem],
        out_specs=(vmem, hbm),
        scratch_shapes=[
            pltpu.VMEM((n_tp, rows, feats), BF16),
            pltpu.VMEM((4, n_kv * w_key.shape[0], width), BF16),
            pltpu.VMEM((n_tp, width, feats), BF16),
            pltpu.VMEM((seqs * hd, width), F32),
            pltpu.VMEM((rows, n_tp * feats), BF16),
            pltpu.VMEM((width // 128, seqs * pad, 128), F32),
            pltpu.VMEM((width // 128, seqs * pad, 128), F32),
            pltpu.VMEM((width // 128, seqs * pad, 128), F32),
            pltpu.VMEM((width // 128, seqs * pad, 128), F32),
            pltpu.VMEM((seqs, width), F32),
            pltpu.VMEM((width // 128, rows, 128), F32),
            pltpu.VMEM((width // 128, rows, 128), F32),
            pltpu.VMEM((4, width // 128, rows, 128), F32),
            pltpu.VMEM((n_tp - 1, rows, feats), BF16),
            pltpu.VMEM((n_tp - 1, rows, feats), BF16),
            dma((2,)),
            dma((6,)),
            dma((n_mat, n_kv)),
            dma((n_mat, n_kv)),
            dma((n_mat, n_kv)),
            dma((max(n_grp - 1, 1), n_mat, n_kv)),
            dma((max(n_grp - 1, 1), n_mat, n_kv)),
            dma((n_tp - 1,)),
            dma((n_tp - 1,)),
            dma((n_tp - 1,)),
            dma((n_tp - 1,)),
            dma(()),
        ],
        compiler_params=pltpu.CompilerParams(
            collective_id=0, has_side_effects=True, vmem_limit_bytes=48 * 2**20),
    )(
        tokens.reshape(rows, feats), in_gain.reshape(1, -1), w_query, w_key, w_value, w_gate,
        w_beta, w_decay, decay_base, out_gain.reshape(1, -1), w_out,
        state.reshape(seqs * hd, width), prev_keys.reshape(rows, width),
        prev_values.reshape(rows, width), prev_beta, prev_decay, accepted.reshape(seqs, 1),
    )
    return mixed.reshape(seqs, props, feats), new_state.reshape(seqs, hd, width)


def solution(mesh):
    sizes = (mesh.shape["grp"], mesh.shape["kv"], mesh.shape["tp"])
    tokens = P(("grp", "kv"), None, "tp")
    placed = (
        tokens, P(), P("kv", "tp"), P("kv", "tp"), P("kv", "tp"), P("kv", "tp"), P(), P(),
        P("tp"), P(), P("tp", "kv"), tokens, tokens, tokens, tokens, tokens, P(("grp", "kv")),
    )
    return jax.shard_map(
        functools.partial(body, sizes),
        mesh=mesh,
        in_specs=placed,
        out_specs=(tokens, tokens),
        check_vma=False,
    )
```

time: 193 us -> 87.1 us (0.45)
  waiting for transfers between devices: 77.1 us -> 0 us
  Pallas kernels: 0 us -> 68.2 us
  matrix products: 41.6 us -> 0 us
  local copies, waits for them, and re-layouts: 40.1 us -> 17.6 us
  between operations: 14.6 us -> 0.68 us
  other arithmetic: 9.67 us -> 0 us
  blocking collectives: 8.86 us -> 0 us
    pallas_call x0 -> x1, Pallas kernels: none -> 68.2 us  [body(): pl.pallas_call(functools.partial(kernel, cfg), out_shape=(jax.ShapeDtypeS...]
    all_gather x5 -> x0, waiting for transfers between devices: 65.8 us -> none  [the longest x1 26 us: body(): key_vec = add_rows(lax.all_gather(w_key, 'kv', axis=0, tiled=True))]
    dot_general x15 -> x0, matrix products: 41.6 us -> none  [the longest x2 13.7 us: delta_block(): jnp.einsum('bhpk,bhkv->bhpv', solution[..., value_size:], saved, precisio...]
    unnamed x30 -> x23, local copies, waits for them, and re-layouts: 0.08 us -> 12.6 us
    slice x15 -> x0, local copies, waits for them, and re-layouts: 10.7 us -> none  [the longest x14 10.5 us: delta_block(): lower_mat[:, :, row_index, col_index, None] * solved[col_index]]
    all_gather x1 -> x0, blocking collectives: 8.86 us -> none  [body(): whole = lax.all_gather(tokens, 'tp', axis=2, tiled=True)]
    reduce_scatter x1 -> x0, waiting for transfers between devices: 8.14 us -> none  [body(): lax.psum_scatter(terms.astype(jnp.bfloat16), 'tp', scatter_dimension=1, t...]
    add x1 -> x0, local copies, waits for them, and re-layouts: 7.78 us -> none  [delta_block(): jnp.exp(cumul[..., -1])[..., None, None] * saved]
  transfers between devices with their start and end apart: 6 -> 0, of which waited for: 4 -> 0; matrix products, arithmetic and copies ran while one was open for 45% -> 0% of each run, Pallas kernels for 0% -> 0%
where the time goes in v1:
time: 87.1 us; the launch traced here: 86.5 us
  Pallas kernels  68.2 us (78%)
  local copies, waits for them, and re-layouts  17.6 us (20%)
    pallas_call x1, Pallas kernels, body(): pl.pallas_call(functools.partial(kernel, cfg), out_shape=(jax.ShapeDtypeS...  68.2 us
    unnamed x23, local copies, waits for them, and re-layouts  12.6 us

profile of v1, /device:TPU:0, one launch (start us, length us, event | category | flops | bytes accessed | tf_op | source)
XLA Modules:
  0.0 86.5 jit_solution(6505675649554954233)
XLA Ops:
  0.6 0.7 copy.23.acc_ref
  1.4 0.9 reshape.35.pk_ref
  2.2 0.9 reshape.36.pv_ref
  3.1 0.8 copy.21.pb_ref
  3.9 0.8 copy.22.pd_ref
  4.7 0.9 %reshape.31.tok_hbm = bf16[128,512]{1,0:T(8,128)(2,1)S(1)} reshape(bf16[32,4,512]{2,1,0:T(4,128)(2,1)} %param.17) | data formatting | bytes 262144 | tf_op jit(solution)/shard_map/reshape | solution.py:478
  5.6 1.1 %copy.19.wb_ref = bf16[2048,16]{1,0:T(8,128)(2,1)S(1)} copy(bf16[2048,16]{0,1:T(8,128)(2,1)} %param.23) | data formatting | bytes 131072 | tf_op args[6]
  6.8 1.1 %copy.20.wd_ref = bf16[2048,16]{1,0:T(8,128)(2,1)S(1)} copy(bf16[2048,16]{0,1:T(8,128)(2,1)} %param.24) | data formatting | bytes 131072 | tf_op args[7]
  7.9 0.0 copy-start
  7.9 0.9 %copy-done = bf16[512,256]{1,0:T(8,128)(2,1)S(1)} copy-done((bf16[512,256]{1,0:T(8,128)(2,1)S(1)}, bf16[512,256]{1,0:T(8,128)(2,1)}, u32[]{:S(2)}) %copy-start) | copy-done | bytes 262168
  8.8 0.0 copy-start.1
  8.8 0.9 %copy-done.1 = bf16[512,256]{1,0:T(8,128)(2,1)S(1)} copy-done((bf16[512,256]{1,0:T(8,128)(2,1)S(1)}, bf16[512,256]{1,0:T(8,128)(2,1)}, u32[]{:S(2)}) %copy-start.1) | copy-done | bytes 262168
  9.8 0.0 copy-start.2
  9.8 0.9 %copy-done.2 = bf16[512,256]{1,0:T(8,128)(2,1)S(1)} copy-done((bf16[512,256]{1,0:T(8,128)(2,1)S(1)}, bf16[512,256]{1,0:T(8,128)(2,1)}, u32[]{:S(2)}) %copy-start.2) | copy-done | bytes 262168
  10.7 0.0 copy-start.3
  10.7 0.9 %copy-done.3 = bf16[512,256]{1,0:T(8,128)(2,1)S(1)} copy-done((bf16[512,256]{1,0:T(8,128)(2,1)S(1)}, bf16[512,256]{1,0:T(8,128)(2,1)}, u32[]{:S(2)}) %copy-start.3) | copy-done | bytes 262168
  11.7 0.0 copy-start.4
  11.7 0.9 %copy-done.4 = bf16[256,512]{1,0:T(8,128)(2,1)S(1)} copy-done((bf16[256,512]{1,0:T(8,128)(2,1)S(1)}, bf16[256,512]{1,0:T(8,128)(2,1)}, u32[]{:S(2)}) %copy-start.4) | copy-done | bytes 262168
  12.6 0.0 copy-start.6
  12.6 0.7 copy-done.6
  13.3 0.0 copy-start.7
  13.3 0.7 copy-done.7
  14.0 0.0 copy-start.8
  14.0 0.7 copy-done.8
  14.7 68.2 %shard_map.176 = (bf16[128,512]{1,0:T(8,128)(2,1)S(1)}, f32[2048,256]{1,0:T(8,128)S(1)}) custom-call(bf16[128,512]{1,0:T(8,128)(2,1)S(1)} %reshape.31.tok_hbm, f32[1,2048]{1,0:T(1,128)S(1)} %bitcast.6, bf16[512,256]{1,0:T(8,128)(2,1)S(1)} %copy-done, bf16[512,256]{1,0:T(8,128)(2,1)S(1)} %copy-done.1, bf16[512,256]{1,0:T(8,128)(2,1)S(1)} %copy-done.2, ...), custom_call_target="tpu_custom_call" | custom-call | tf_op jit(solution)/shard_map/pallas_call | solution.py:437
  82.9 0.0 copy-start.5
  82.9 0.6 copy-done.5
  83.5 1.6 %reshape.38 = bf16[32,4,512]{2,1,0:T(4,128)(2,1)} reshape(bf16[128,512]{1,0:T(8,128)(2,1)} %copy-done.5) | data formatting | bytes 262144 | tf_op jit(solution)/shard_map/reshape | solution.py:483
  85.1 1.3 %copy.25 = f32[32,64,256]{2,1,0:T(8,128)} copy(f32[32,64,256]{2,1,0:T(8,128)S(1)} %bitcast.5) | data formatting | bytes 4194304
Async XLA Ops:
  7.9 1.0 %copy-start = (bf16[512,256]{1,0:T(8,128)(2,1)S(1)}, bf16[512,256]{1,0:T(8,128)(2,1)}, u32[]{:S(2)}) copy-start(bf16[512,256]{1,0:T(8,128)(2,1)} %wq_hbm.1) | copy-start | bytes 786436
  8.8 0.9 %copy-start.1 = (bf16[512,256]{1,0:T(8,128)(2,1)S(1)}, bf16[512,256]{1,0:T(8,128)(2,1)}, u32[]{:S(2)}) copy-start(bf16[512,256]{1,0:T(8,128)(2,1)} %wk_hbm.1) | copy-start | bytes 786436
  9.8 0.9 %copy-start.2 = (bf16[512,256]{1,0:T(8,128)(2,1)S(1)}, bf16[512,256]{1,0:T(8,128)(2,1)}, u32[]{:S(2)}) copy-start(bf16[512,256]{1,0:T(8,128)(2,1)} %wv_hbm.1) | copy-start | bytes 786436
  10.7 0.9 %copy-start.3 = (bf16[512,256]{1,0:T(8,128)(2,1)S(1)}, bf16[512,256]{1,0:T(8,128)(2,1)}, u32[]{:S(2)}) copy-start(bf16[512,256]{1,0:T(8,128)(2,1)} %wg_hbm.1) | copy-start | bytes 786436
  11.7 0.9 %copy-start.4 = (bf16[256,512]{1,0:T(8,128)(2,1)S(1)}, bf16[256,512]{1,0:T(8,128)(2,1)}, u32[]{:S(2)}) copy-start(bf16[256,512]{1,0:T(8,128)(2,1)} %wo_hbm.1) | copy-start | bytes 786436
  12.6 0.7 copy-start.6
  13.3 0.7 copy-start.7
  14.0 0.7 copy-start.8
  82.9 0.7 copy-start.5

commit v2 on v1

--- a/solution.py
+++ b/solution.py
@@ -15,12 +15,12 @@
 
 def kernel(
     cfg,
-    tok_hbm, gain_ref, wq_hbm, wk_hbm, wv_hbm, wg_hbm, wb_ref, wd_ref, base_ref, og_ref, wo_hbm,
-    state_hbm, pk_ref, pv_ref, pb_ref, pd_ref, acc_ref,
+    tok_hbm, gain_hbm, wq_hbm, wk_hbm, wv_hbm, wg_hbm, wb_hbm, wd_hbm, base_hbm, og_hbm, wo_hbm,
+    state_hbm, pk_hbm, pv_hbm, pb_hbm, pd_hbm, acc_hbm,
     mixed_ref, new_hbm,
-    tok, wp, wo, st, normed, kq, res, tk, up, al, rows_a, rows_b, proj, send_buf, recv_buf,
+    gain_ref, wb_ref, wd_ref, base_ref, og_ref, pk_ref, pv_ref, pb_ref, pd_ref, acc_ref, tok, wp, wo, st, normed, kq, res, tk, up, al, rows_a, rows_b, proj, send_buf, recv_buf, gate_buf, own_share,
     in_sem, own_sem, zr_send, zl_send, z_recv, y_send, y_recv, t_send, t_recv, r_send, r_recv,
-    out_sem,
+    out_sem, small_sem,
 ):
     n_grp, n_kv, n_tp, seqs, props, heads, hd, gather_out = cfg
     width = heads * hd
@@ -45,6 +45,17 @@
             copy = pltpu.make_async_copy(wo_hbm, wo.at[k], own_sem.at[m])
         copy.start()
         own_copies.append(copy)
+    early, late = [], []
+    pairs = [
+        (pk_hbm, pk_ref, early), (pv_hbm, pv_ref, early), (pb_hbm, pb_ref, early),
+        (pd_hbm, pd_ref, early), (acc_hbm, acc_ref, early), (gain_hbm, gain_ref, late),
+        (wb_hbm, wb_ref, late), (wd_hbm, wd_ref, late), (base_hbm, base_ref, late),
+        (og_hbm, og_ref, late),
+    ]
+    for i, (src, dst, group) in enumerate(pairs):
+        copy = pltpu.make_async_copy(src, dst, small_sem.at[i])
+        copy.start()
+        group.append(copy)
     state_in = pltpu.make_async_copy(state_hbm, st, in_sem.at[1])
     state_in.start()
     out_in = None
@@ -113,33 +124,35 @@
         def _():
             z_left(m, k).start()
 
+    def forward_step(m, s):
+        left = k - 1 - s
+        right = k + 1 + s
+
+        @pl.when(left >= 0)
+        def _():
+            z_right(m, left).wait_recv()
+
+            @pl.when(k < n_kv - 1)
+            def _():
+                z_right(m, left).start()
+
+            for d in range(1, n_grp):
+                y_copy(m, left, d).start()
+
+        @pl.when(right < n_kv)
+        def _():
+            z_left(m, right).wait_recv()
+
+            @pl.when(k > 0)
+            def _():
+                z_left(m, right).start()
+
+            for d in range(1, n_grp):
+                y_copy(m, right, d).start()
+
     def forward(m):
         def step(s, carry):
-            left = k - 1 - s
-            right = k + 1 + s
-
-            @pl.when(left >= 0)
-            def _():
-                z_right(m, left).wait_recv()
-
-                @pl.when(k < n_kv - 1)
-                def _():
-                    z_right(m, left).start()
-
-                for d in range(1, n_grp):
-                    y_copy(m, left, d).start()
-
-            @pl.when(right < n_kv)
-            def _():
-                z_left(m, right).wait_recv()
-
-                @pl.when(k > 0)
-                def _():
-                    z_left(m, right).start()
-
-                for d in range(1, n_grp):
-                    y_copy(m, right, d).start()
-
+            forward_step(m, s)
             return carry
 
         lax.fori_loop(0, n_kv - 1, step, 0)
@@ -196,12 +209,6 @@
             ref[(*lead, c, at)] = x[:, c * lanes : (c + 1) * lanes]
 
     every = pl.ds(0, rows)
-
-    def spread(x):
-        total = jnp.zeros((x.shape[0], width), F32)
-        for h in range(heads):
-            total = jnp.where(lane_head == h, x[:, h : h + 1], total)
-        return total
 
     pad = 2 * props
 
@@ -251,17 +258,28 @@
     def split(ref):
         return [rd(ref, pl.ds(t, seqs, stride=props)) for t in range(props)]
 
-    pk = pk_ref[...].astype(F32)
+    for copy in early:
+        copy.wait()
+    pk = pk_ref[...].astype(F32).reshape(rows, width)
     wr(rows_a, every, pk * lax.rsqrt(head_sum(pk * pk) + EPS))
-    wr(rows_b, every, pv_ref[...].astype(F32))
+    wr(rows_b, every, pv_ref[...].astype(F32).reshape(rows, width))
     keys = split(rows_a)
     values = split(rows_b)
-    accepted = jnp.broadcast_to(acc_ref[...], (seqs, width))
+    own_head = (
+        lax.broadcasted_iota(jnp.int32, (heads, width), 0)
+        == lax.broadcasted_iota(jnp.int32, (heads, width), 1) // hd
+    ).astype(F32)
+
+    def over_lanes(x):
+        return lax.dot_general(
+            x, own_head, (((0,), (0,)), ((), ())),
+            precision=lax.Precision.HIGHEST, preferred_element_type=F32)
+
     weights, logs = [], []
     for t in range(props):
-        live = (accepted > t).astype(F32)
-        weights.append(spread(jax.nn.sigmoid(pb_ref[:, t, :])) * live)
-        logs.append(spread(pd_ref[:, t, :]) * live)
+        live = (acc_ref[...] > t).astype(F32)
+        weights.append(over_lanes(jax.nn.sigmoid(pb_ref[t]) * live))
+        logs.append(over_lanes(pd_ref[t] * live))
         wr(kq, pl.ds(t, seqs, stride=pad), keys[t])
         wr(kq, pl.ds(props + t, seqs, stride=pad), keys[t])
     state_in.wait()
@@ -291,30 +309,33 @@
 
     for d in range(1, n_tp):
         t_wait(d)
+    for copy in late:
+        copy.wait()
     square = jnp.zeros((rows, 1), F32)
     for i in range(n_tp):
-        wide = tok[i].astype(F32)
+        wide = tok[i].astype(F32).reshape(rows, -1)
         square = square + jnp.sum(wide * wide, -1, keepdims=True)
-    feats = tok.shape[2]
+    feats = tok.shape[3]
     scale = lax.rsqrt(square / (n_tp * feats) + EPS)
     for i in range(n_tp):
         cols = slice(i * feats, (i + 1) * feats)
-        normed[:, cols] = (tok[i].astype(F32) * scale * gain_ref[:, cols]).astype(BF16)
-    all_heads = wb_ref.shape[1]
+        normed[:, cols] = (tok[i].astype(F32).reshape(rows, -1) * scale * gain_ref[:, cols]).astype(BF16)
+    all_heads = wb_ref.shape[0]
     pick = (
         lax.broadcasted_iota(jnp.int32, (all_heads, width), 0)
         == t_me * heads + lax.broadcasted_iota(jnp.int32, (all_heads, width), 1) // hd
     ).astype(F32)
 
     def per_head(ref):
-        raw = jnp.dot(normed[...], ref[...], preferred_element_type=F32)
+        raw = lax.dot_general(
+            normed[...], ref[...], (((1,), (1,)), ((), ())), preferred_element_type=F32)
         return jnp.dot(raw, pick, precision=lax.Precision.HIGHEST, preferred_element_type=F32)
 
     wr(rows_a, every, jax.nn.sigmoid(per_head(wb_ref)))
     weights = split(rows_a)
     base = jnp.zeros((1, width), F32)
     for h in range(heads):
-        base = jnp.where(lane_head == h, base_ref[h], base)
+        base = jnp.where(lane_head == h, base_ref[:, h : h + 1], base)
     wr(rows_b, every, -base * jax.nn.softplus(per_head(wd_ref)))
     logs = split(rows_b)
 
@@ -332,7 +353,29 @@
             wr(proj, every, value, m)
 
     outs = None
-    for m in range(n_mat):
+    def r_copy(dest):
+        return pltpu.make_async_remote_copy(
+            send_buf.at[dest], recv_buf.at[t_me], r_send.at[dest], r_recv.at[t_me],
+            device_id={"tp": dest}, device_id_type=MESH)
+
+    def r_wait(origin):
+        pltpu.make_async_remote_copy(
+            send_buf.at[origin], recv_buf.at[origin], r_send.at[origin], r_recv.at[origin],
+            device_id={"tp": origin}, device_id_type=MESH).wait_recv()
+
+    def send_share(dest):
+        share = jnp.dot(gate_buf[...], wo[dest], preferred_element_type=F32)
+
+        @pl.when(dest == t_me)
+        def _():
+            own_share[...] = share
+
+        @pl.when(dest != t_me)
+        def _():
+            send_buf[dest] = share.astype(BF16)
+            r_copy(dest).start()
+
+    for m in range(len(sources)):
         if m >= 1 and m + 1 < n_mat:
             send_own(m + 1)
         forward(m)
@@ -359,34 +402,49 @@
                 jnp.broadcast_to(og_ref[...], (8, hd)), tile_gain,
                 precision=lax.Precision.HIGHEST, preferred_element_type=F32)[:1]
             wr(rows_a, every, out * gain)
-    if not gather_out:
-        finish(n_mat - 1)
+    finish(len(sources) - 1)
+    gate = rd(proj, every, 3)
+    gate_buf[...] = (rd(rows_a, every) * (gate / (1.0 + jnp.exp(-gate)))).astype(BF16)
+    if gather_out:
+        m = n_mat - 1
+
+        def take(s, carry):
+            @pl.when(s < n_kv - 1)
+            def _():
+                forward_step(m, s)
+
+            @pl.when(k - s >= 0)
+            def _():
+                @pl.when(s > 0)
+                def _():
+                    for d in range(1, n_grp):
+                        y_wait(m, k - s, d)
+
+                send_share(k - s)
+
+            @pl.when(jnp.logical_and(s > 0, k + s < n_kv))
+            def _():
+                for d in range(1, n_grp):
+                    y_wait(m, k + s, d)
+                send_share(k + s)
+
+            return carry
+
+        lax.fori_loop(0, n_kv, take, 0)
+    else:
         out_in.wait()
-    gate = rd(proj, every, 3)
-    gated = (rd(rows_a, every) * (gate / (1.0 + jnp.exp(-gate)))).astype(BF16)
-    if gather_out:
-        finish(n_mat - 1)
-
-    def r_copy(d):
-        dest = lax.rem(t_me + d, n_tp)
-        return pltpu.make_async_remote_copy(
-            send_buf.at[d - 1], recv_buf.at[d - 1], r_send.at[d - 1], r_recv.at[d - 1],
-            device_id={"tp": dest}, device_id_type=MESH)
-
-    order = sorted(range(1, n_tp), key=lambda d: -min(d, n_tp - d))
-    for d in order:
-        dest = lax.rem(t_me + d, n_tp)
-        send_buf[d - 1] = jnp.dot(gated, wo[dest], preferred_element_type=F32).astype(BF16)
-        r_copy(d).start()
-    total = jnp.dot(gated, wo[t_me], preferred_element_type=F32)
-    for d in reversed(order):
-        r_copy(d).wait_recv()
-        total = total + recv_buf[d - 1].astype(F32)
-    mixed_ref[...] = total.astype(BF16)
+        for d in range(n_tp):
+            send_share(lax.rem(t_me + d, n_tp))
+    total = own_share[...]
+    for d in range(1, n_tp):
+        origin = lax.rem(t_me + d, n_tp)
+        r_wait(origin)
+        total = total + recv_buf[origin].astype(F32)
+    mixed_ref[...] = total.reshape(seqs, props, feats).astype(BF16)
 
     for d in range(1, n_tp):
         t_copy(d).wait_send()
-        r_copy(d).wait_send()
+        r_copy(lax.rem(t_me + d, n_tp)).wait_send()
 
     def drain(m):
         def step(o, carry):
@@ -432,19 +490,25 @@
     cfg = (n_grp, n_kv, n_tp, seqs, props, heads, hd, gather_out)
     vmem = pl.BlockSpec(memory_space=pltpu.VMEM)
     hbm = pl.BlockSpec(memory_space=pl.ANY)
-    smem = pl.BlockSpec(memory_space=pltpu.SMEM)
+    args = (
+        tokens, in_gain.reshape(1, -1), w_query, w_key, w_value, w_gate,
+        w_beta.T, w_decay.T, decay_base.reshape(1, -1), out_gain.reshape(1, -1), w_out,
+        state.reshape(seqs * hd, width), prev_keys, prev_values,
+        jnp.transpose(prev_beta, (1, 2, 0)), jnp.transpose(prev_decay, (1, 2, 0)),
+        accepted.reshape(1, seqs),
+    )
     dma = pltpu.SemaphoreType.DMA
     mixed, new_state = pl.pallas_call(
         functools.partial(kernel, cfg),
         out_shape=(
-            jax.ShapeDtypeStruct((rows, feats), BF16),
+            jax.ShapeDtypeStruct((seqs, props, feats), BF16),
             jax.ShapeDtypeStruct((seqs * hd, width), F32),
         ),
-        in_specs=[hbm, vmem, hbm, hbm, hbm, hbm, vmem, vmem, smem, vmem, hbm, hbm,
-                  vmem, vmem, vmem, vmem, vmem],
+        in_specs=[hbm] * len(args),
         out_specs=(vmem, hbm),
         scratch_shapes=[
-            pltpu.VMEM((n_tp, rows, feats), BF16),
+            *[pltpu.VMEM(args[i].shape, args[i].dtype) for i in (1, 6, 7, 8, 9, 12, 13, 14, 15, 16)],
+            pltpu.VMEM((n_tp, seqs, props, feats), BF16),
             pltpu.VMEM((4, n_kv * w_key.shape[0], width), BF16),
             pltpu.VMEM((n_tp, width, feats), BF16),
             pltpu.VMEM((seqs * hd, width), F32),
@@ -457,8 +521,10 @@
             pltpu.VMEM((width // 128, rows, 128), F32),
             pltpu.VMEM((width // 128, rows, 128), F32),
             pltpu.VMEM((4, width // 128, rows, 128), F32),
-            pltpu.VMEM((n_tp - 1, rows, feats), BF16),
-            pltpu.VMEM((n_tp - 1, rows, feats), BF16),
+            pltpu.VMEM((n_tp, rows, feats), BF16),
+            pltpu.VMEM((n_tp, rows, feats), BF16),
+            pltpu.VMEM((rows, width), BF16),
+            pltpu.VMEM((rows, feats), F32),
             dma((2,)),
             dma((6,)),
             dma((n_mat, n_kv)),
@@ -468,19 +534,15 @@
             dma((max(n_grp - 1, 1), n_mat, n_kv)),
             dma((n_tp - 1,)),
             dma((n_tp - 1,)),
-            dma((n_tp - 1,)),
-            dma((n_tp - 1,)),
+            dma((n_tp,)),
+            dma((n_tp,)),
             dma(()),
+            dma((10,)),
         ],
         compiler_params=pltpu.CompilerParams(
-            collective_id=0, has_side_effects=True, vmem_limit_bytes=48 * 2**20),
-    )(
-        tokens.reshape(rows, feats), in_gain.reshape(1, -1), w_query, w_key, w_value, w_gate,
-        w_beta, w_decay, decay_base, out_gain.reshape(1, -1), w_out,
-        state.reshape(seqs * hd, width), prev_keys.reshape(rows, width),
-        prev_values.reshape(rows, width), prev_beta, prev_decay, accepted.reshape(seqs, 1),
-    )
-    return mixed.reshape(seqs, props, feats), new_state.reshape(seqs, hd, width)
+            collective_id=0, has_side_effects=True, vmem_limit_bytes=67043328),
+    )(*args)
+    return mixed, new_state.reshape(seqs, hd, width)
 
 
 def solution(mesh):

time: 87.1 us -> 73.1 us (0.84)
  local copies, waits for them, and re-layouts: 17.6 us -> 4.73 us
    unnamed x23 -> x2, local copies, waits for them, and re-layouts: 12.6 us -> 4.73 us
    reshape x5 -> x0, local copies, waits for them, and re-layouts: 5 us -> none  [the longest x1 1.59 us: body(): mixed.reshape(seqs, props, feats)]
where the time goes in v2:
time: 73.1 us; the launch traced here: 73 us
  Pallas kernels  67.6 us (92%)
  local copies, waits for them, and re-layouts  4.73 us (6%)
    pallas_call x1, Pallas kernels, body(): pl.pallas_call(functools.partial(kernel, cfg), out_shape=(jax.ShapeDtypeS...  67.6 us
    unnamed x2, local copies, waits for them, and re-layouts  4.73 us

profile of v2, /device:TPU:0, one launch (start us, length us, event | category | flops | bytes accessed | tf_op | source)
XLA Modules:
  0.0 73.0 jit_solution(17150958701875720667)
XLA Ops:
  0.6 67.6 %shard_map.176 = (bf16[32,4,512]{2,1,0:T(4,128)(2,1)}, f32[2048,256]{1,0:T(8,128)}) custom-call(bf16[32,4,512]{2,1,0:T(4,128)(2,1)} %tok_hbm.1, f32[1,2048]{1,0:T(1,128)} %bitcast.14, bf16[512,256]{1,0:T(8,128)(2,1)} %wq_hbm.1, bf16[512,256]{1,0:T(8,128)(2,1)} %wk_hbm.1, bf16[512,256]{1,0:T(8,128)(2,1)} %wv_hbm.1, bf16[512,256]{1,0:T(8,128)(2,1)} %wg_hbm.1, ...), custom_call_target="tpu_custom_call" | custom-call | tf_op jit(solution)/shard_map/pallas_call | solution.py:501
  68.2 1.6 %copy.21 = bf16[32,4,512]{2,1,0:T(4,128)(2,1)} copy(bf16[32,4,512]{2,1,0:T(4,128)(2,1)} %get-tuple-element.8) | data formatting | bytes 262144
  69.9 3.1 %copy.22 = f32[32,64,256]{2,1,0:T(8,128)} copy(f32[32,64,256]{2,1,0:T(8,128)} %bitcast.11) | data formatting | bytes 4194304

commit v3 on v2

--- a/solution.py
+++ b/solution.py
@@ -17,10 +17,10 @@
     cfg,
     tok_hbm, gain_hbm, wq_hbm, wk_hbm, wv_hbm, wg_hbm, wb_hbm, wd_hbm, base_hbm, og_hbm, wo_hbm,
     state_hbm, pk_hbm, pv_hbm, pb_hbm, pd_hbm, acc_hbm,
-    mixed_ref, new_hbm,
-    gain_ref, wb_ref, wd_ref, base_ref, og_ref, pk_ref, pv_ref, pb_ref, pd_ref, acc_ref, tok, wp, wo, st, normed, kq, res, tk, up, al, rows_a, rows_b, proj, send_buf, recv_buf, gate_buf, own_share,
+    mixed_ref, st,
+    gain_ref, wb_ref, wd_ref, base_ref, og_ref, pk_ref, pv_ref, pb_ref, pd_ref, acc_ref, tok, wp, wo, normed, kq, res, tk, up, al, rows_a, rows_b, proj, send_buf, recv_buf, gate_buf, own_share,
     in_sem, own_sem, zr_send, zl_send, z_recv, y_send, y_recv, t_send, t_recv, r_send, r_recv,
-    out_sem, small_sem,
+    small_sem,
 ):
     n_grp, n_kv, n_tp, seqs, props, heads, hd, gather_out = cfg
     width = heads * hd
@@ -184,6 +184,7 @@
     for d in range(1, n_tp):
         t_copy(d).start()
     send_own(1)
+    send_own(2)
 
     blk = (
         lax.broadcasted_iota(jnp.int32, (width, width), 0) // hd
@@ -303,9 +304,13 @@
         st[where, :] = tile
         return carry
 
-    lax.fori_loop(0, seqs, renew, 0, unroll=2)
-    state_out = pltpu.make_async_copy(st, new_hbm, out_sem)
-    state_out.start()
+    forward(0)
+    send_own(3)
+    lax.fori_loop(0, seqs // 2, renew, 0, unroll=2)
+    forward(1)
+    if gather_out:
+        send_own(n_mat - 1)
+    lax.fori_loop(seqs // 2, seqs, renew, 0, unroll=2)
 
     for d in range(1, n_tp):
         t_wait(d)
@@ -376,9 +381,8 @@
             r_copy(dest).start()
 
     for m in range(len(sources)):
-        if m >= 1 and m + 1 < n_mat:
-            send_own(m + 1)
-        forward(m)
+        if m >= 2:
+            forward(m)
         if m >= 1:
             finish(m - 1)
         if m == 3:
@@ -467,7 +471,6 @@
 
     for m in range(n_mat):
         drain(m)
-    state_out.wait()
 
 
 def body(
@@ -489,7 +492,7 @@
     n_mat = 5 if gather_out else 4
     cfg = (n_grp, n_kv, n_tp, seqs, props, heads, hd, gather_out)
     vmem = pl.BlockSpec(memory_space=pltpu.VMEM)
-    hbm = pl.BlockSpec(memory_space=pl.ANY)
+    hbm = pl.BlockSpec(memory_space=pltpu.HBM)
     args = (
         tokens, in_gain.reshape(1, -1), w_query, w_key, w_value, w_gate,
         w_beta.T, w_decay.T, decay_base.reshape(1, -1), out_gain.reshape(1, -1), w_out,
@@ -505,13 +508,12 @@
             jax.ShapeDtypeStruct((seqs * hd, width), F32),
         ),
         in_specs=[hbm] * len(args),
-        out_specs=(vmem, hbm),
+        out_specs=(vmem, vmem),
         scratch_shapes=[
             *[pltpu.VMEM(args[i].shape, args[i].dtype) for i in (1, 6, 7, 8, 9, 12, 13, 14, 15, 16)],
             pltpu.VMEM((n_tp, seqs, props, feats), BF16),
             pltpu.VMEM((4, n_kv * w_key.shape[0], width), BF16),
             pltpu.VMEM((n_tp, width, feats), BF16),
-            pltpu.VMEM((seqs * hd, width), F32),
             pltpu.VMEM((rows, n_tp * feats), BF16),
             pltpu.VMEM((width // 128, seqs * pad, 128), F32),
             pltpu.VMEM((width // 128, seqs * pad, 128), F32),
@@ -536,11 +538,10 @@
             dma((n_tp - 1,)),
             dma((n_tp,)),
             dma((n_tp,)),
-            dma(()),
             dma((10,)),
         ],
         compiler_params=pltpu.CompilerParams(
-            collective_id=0, has_side_effects=True, vmem_limit_bytes=67043328),
+            collective_id=0, has_side_effects=True, vmem_limit_bytes=48 * 2**20),
     )(*args)
     return mixed, new_state.reshape(seqs, hd, width)
 

time: 73.1 us -> 85.4 us (1.17)
  local copies, waits for them, and re-layouts: 4.73 us -> 16.6 us
    unnamed x2 -> x36, local copies, waits for them, and re-layouts: 4.73 us -> 16.6 us
where the time goes in v3:
time: 85.4 us; the launch traced here: 84.7 us
  Pallas kernels  67.4 us (79%)
  local copies, waits for them, and re-layouts  16.6 us (19%)
    pallas_call x1, Pallas kernels, body(): pl.pallas_call(functools.partial(kernel, cfg), out_shape=(jax.ShapeDtypeS...  67.4 us
    unnamed x36, local copies, waits for them, and re-layouts  16.6 us

profile of v3, /device:TPU:0, one launch (start us, length us, event | category | flops | bytes accessed | tf_op | source)
XLA Modules:
  0.0 84.7 jit_solution(14271192994871514970)
XLA Ops:
  0.6 0.0 copy-start
  0.6 1.6 %copy-done = f32[32,64,256]{2,1,0:T(8,128)S(1)} copy-done((f32[32,64,256]{2,1,0:T(8,128)S(1)}, f32[32,64,256]{2,1,0:T(8,128)}, u32[]{:S(2)}) %copy-start) | copy-done | bytes 2097176
  2.2 0.0 copy-start.1
  2.2 0.9 %copy-done.1 = bf16[512,256]{1,0:T(8,128)(2,1)S(1)} copy-done((bf16[512,256]{1,0:T(8,128)(2,1)S(1)}, bf16[512,256]{1,0:T(8,128)(2,1)}, u32[]{:S(2)}) %copy-start.1) | copy-done | bytes 262168
  3.2 0.0 copy-start.2
  3.2 0.9 %copy-done.2 = bf16[512,256]{1,0:T(8,128)(2,1)S(1)} copy-done((bf16[512,256]{1,0:T(8,128)(2,1)S(1)}, bf16[512,256]{1,0:T(8,128)(2,1)}, u32[]{:S(2)}) %copy-start.2) | copy-done | bytes 262168
  4.1 0.0 copy-start.3
  4.1 0.9 %copy-done.3 = bf16[512,256]{1,0:T(8,128)(2,1)S(1)} copy-done((bf16[512,256]{1,0:T(8,128)(2,1)S(1)}, bf16[512,256]{1,0:T(8,128)(2,1)}, u32[]{:S(2)}) %copy-start.3) | copy-done | bytes 262168
  5.1 0.0 copy-start.4
  5.1 0.9 %copy-done.4 = bf16[512,256]{1,0:T(8,128)(2,1)S(1)} copy-done((bf16[512,256]{1,0:T(8,128)(2,1)S(1)}, bf16[512,256]{1,0:T(8,128)(2,1)}, u32[]{:S(2)}) %copy-start.4) | copy-done | bytes 262168
  6.0 0.0 copy-start.5
  6.0 0.9 %copy-done.5 = bf16[256,512]{1,0:T(8,128)(2,1)S(1)} copy-done((bf16[256,512]{1,0:T(8,128)(2,1)S(1)}, bf16[256,512]{1,0:T(8,128)(2,1)}, u32[]{:S(2)}) %copy-start.5) | copy-done | bytes 262168
  7.0 0.0 copy-start.6
  7.0 0.9 %copy-done.6 = bf16[32,4,512]{2,1,0:T(4,128)(2,1)S(1)} copy-done((bf16[32,4,512]{2,1,0:T(4,128)(2,1)S(1)}, bf16[32,4,512]{2,1,0:T(4,128)(2,1)}, u32[]{:S(2)}) %copy-start.6) | copy-done | bytes 131096
  7.9 0.0 copy-start.7
  7.9 0.8 copy-done.7
  8.7 0.0 copy-start.8
  8.7 0.8 copy-done.8
  9.6 0.0 copy-start.9
  9.6 0.8 copy-done.9
  10.4 0.0 copy-start.10
  10.4 0.8 copy-done.10
  11.2 0.0 copy-start.11
  11.2 0.7 copy-done.11
  11.9 0.7 copy-done.12
  12.6 0.7 copy-done.13
  13.3 0.7 copy-done.14
  14.0 0.7 copy-done.15
  14.7 0.7 copy-done.16
  15.3 67.4 %shard_map.176 = (bf16[32,4,512]{2,1,0:T(4,128)(2,1)S(1)}, f32[2048,256]{1,0:T(8,128)S(1)}) custom-call(bf16[32,4,512]{2,1,0:T(4,128)(2,1)S(1)} %copy-done.6, f32[1,2048]{1,0:T(1,128)S(1)} %bitcast.14, bf16[512,256]{1,0:T(8,128)(2,1)S(1)} %copy-done.1, bf16[512,256]{1,0:T(8,128)(2,1)S(1)} %copy-done.2, bf16[512,256]{1,0:T(8,128)(2,1)S(1)} %copy-done.3, ...), custom_call_target="tpu_custom_call" | custom-call | tf_op jit(solution)/shard_map/pallas_call | solution.py:504
  82.7 0.7 copy.21
  83.4 1.3 %copy.22 = f32[32,64,256]{2,1,0:T(8,128)} copy(f32[32,64,256]{2,1,0:T(8,128)S(1)} %bitcast.11) | data formatting | bytes 4194304
  (5 shorter events, 0.0 us)
Async XLA Ops:
  0.6 1.6 %copy-start = (f32[32,64,256]{2,1,0:T(8,128)S(1)}, f32[32,64,256]{2,1,0:T(8,128)}, u32[]{:S(2)}) copy-start(f32[32,64,256]{2,1,0:T(8,128)} %param.28) | copy-start | bytes 6291460
  2.2 0.9 %copy-start.1 = (bf16[512,256]{1,0:T(8,128)(2,1)S(1)}, bf16[512,256]{1,0:T(8,128)(2,1)}, u32[]{:S(2)}) copy-start(bf16[512,256]{1,0:T(8,128)(2,1)} %wq_hbm.1) | copy-start | bytes 786436
  3.2 0.9 %copy-start.2 = (bf16[512,256]{1,0:T(8,128)(2,1)S(1)}, bf16[512,256]{1,0:T(8,128)(2,1)}, u32[]{:S(2)}) copy-start(bf16[512,256]{1,0:T(8,128)(2,1)} %wk_hbm.1) | copy-start | bytes 786436
  4.1 0.9 %copy-start.3 = (bf16[512,256]{1,0:T(8,128)(2,1)S(1)}, bf16[512,256]{1,0:T(8,128)(2,1)}, u32[]{:S(2)}) copy-start(bf16[512,256]{1,0:T(8,128)(2,1)} %wv_hbm.1) | copy-start | bytes 786436
  5.1 0.9 %copy-start.4 = (bf16[512,256]{1,0:T(8,128)(2,1)S(1)}, bf16[512,256]{1,0:T(8,128)(2,1)}, u32[]{:S(2)}) copy-start(bf16[512,256]{1,0:T(8,128)(2,1)} %wg_hbm.1) | copy-start | bytes 786436
  6.0 0.9 %copy-start.5 = (bf16[256,512]{1,0:T(8,128)(2,1)S(1)}, bf16[256,512]{1,0:T(8,128)(2,1)}, u32[]{:S(2)}) copy-start(bf16[256,512]{1,0:T(8,128)(2,1)} %wo_hbm.1) | copy-start | bytes 786436
  7.0 0.9 %copy-start.6 = (bf16[32,4,512]{2,1,0:T(4,128)(2,1)S(1)}, bf16[32,4,512]{2,1,0:T(4,128)(2,1)}, u32[]{:S(2)}) copy-start(bf16[32,4,512]{2,1,0:T(4,128)(2,1)} %tok_hbm.1) | copy-start | bytes 393220
  7.9 0.8 copy-start.7
  8.7 0.8 copy-start.8
  9.6 0.8 copy-start.9
  10.4 0.8 copy-start.10
  11.2 0.7 copy-start.11
  11.9 0.7 copy-start.12
  12.6 0.7 copy-start.13
  13.3 0.7 copy-start.14
  14.0 0.7 copy-start.15
  14.7 0.7 copy-start.16

commit v4 on v3

--- a/solution.py
+++ b/solution.py
@@ -17,10 +17,10 @@
     cfg,
     tok_hbm, gain_hbm, wq_hbm, wk_hbm, wv_hbm, wg_hbm, wb_hbm, wd_hbm, base_hbm, og_hbm, wo_hbm,
     state_hbm, pk_hbm, pv_hbm, pb_hbm, pd_hbm, acc_hbm,
-    mixed_ref, st,
-    gain_ref, wb_ref, wd_ref, base_ref, og_ref, pk_ref, pv_ref, pb_ref, pd_ref, acc_ref, tok, wp, wo, normed, kq, res, tk, up, al, rows_a, rows_b, proj, send_buf, recv_buf, gate_buf, own_share,
+    mixed_ref, new_hbm,
+    gain_ref, wb_ref, wd_ref, base_ref, og_ref, pk_ref, pv_ref, pb_ref, pd_ref, acc_ref, tok, wp, wo, st, normed, kq, res, tk, up, al, rows_a, rows_b, proj, send_buf, recv_buf, gate_buf, own_share,
     in_sem, own_sem, zr_send, zl_send, z_recv, y_send, y_recv, t_send, t_recv, r_send, r_recv,
-    small_sem,
+    out_sem, small_sem,
 ):
     n_grp, n_kv, n_tp, seqs, props, heads, hd, gather_out = cfg
     width = heads * hd
@@ -311,6 +311,8 @@
     if gather_out:
         send_own(n_mat - 1)
     lax.fori_loop(seqs // 2, seqs, renew, 0, unroll=2)
+    state_out = pltpu.make_async_copy(st, new_hbm, out_sem)
+    state_out.start()
 
     for d in range(1, n_tp):
         t_wait(d)
@@ -471,6 +473,7 @@
 
     for m in range(n_mat):
         drain(m)
+    state_out.wait()
 
 
 def body(
@@ -508,12 +511,13 @@
             jax.ShapeDtypeStruct((seqs * hd, width), F32),
         ),
         in_specs=[hbm] * len(args),
-        out_specs=(vmem, vmem),
+        out_specs=(vmem, pl.BlockSpec(memory_space=pl.ANY)),
         scratch_shapes=[
             *[pltpu.VMEM(args[i].shape, args[i].dtype) for i in (1, 6, 7, 8, 9, 12, 13, 14, 15, 16)],
             pltpu.VMEM((n_tp, seqs, props, feats), BF16),
             pltpu.VMEM((4, n_kv * w_key.shape[0], width), BF16),
             pltpu.VMEM((n_tp, width, feats), BF16),
+            pltpu.VMEM((seqs * hd, width), F32),
             pltpu.VMEM((rows, n_tp * feats), BF16),
             pltpu.VMEM((width // 128, seqs * pad, 128), F32),
             pltpu.VMEM((width // 128, seqs * pad, 128), F32),
@@ -538,10 +542,11 @@
             dma((n_tp - 1,)),
             dma((n_tp,)),
             dma((n_tp,)),
+            dma(()),
             dma((10,)),
         ],
         compiler_params=pltpu.CompilerParams(
-            collective_id=0, has_side_effects=True, vmem_limit_bytes=48 * 2**20),
+            collective_id=0, has_side_effects=True, vmem_limit_bytes=67043328),
     )(*args)
     return mixed, new_state.reshape(seqs, hd, width)
 

time: 85.4 us -> 72.9 us (0.85)
  local copies, waits for them, and re-layouts: 16.6 us -> 4.73 us
    unnamed x36 -> x2, local copies, waits for them, and re-layouts: 16.6 us -> 4.73 us
where the time goes in v4:
time: 72.9 us; the launch traced here: 72.8 us
  Pallas kernels  67.4 us (92%)
  local copies, waits for them, and re-layouts  4.73 us (6%)
    pallas_call x1, Pallas kernels, body(): pl.pallas_call(functools.partial(kernel, cfg), out_shape=(jax.ShapeDtypeS...  67.4 us
    unnamed x2, local copies, waits for them, and re-layouts  4.73 us

profile of v4, /device:TPU:0, one launch (start us, length us, event | category | flops | bytes accessed | tf_op | source)
XLA Modules:
  0.0 72.8 jit_solution(520634901363984867)
XLA Ops:
  0.6 67.4 %shard_map.176 = (bf16[32,4,512]{2,1,0:T(4,128)(2,1)}, f32[2048,256]{1,0:T(8,128)}) custom-call(bf16[32,4,512]{2,1,0:T(4,128)(2,1)} %tok_hbm.1, f32[1,2048]{1,0:T(1,128)} %bitcast.14, bf16[512,256]{1,0:T(8,128)(2,1)} %wq_hbm.1, bf16[512,256]{1,0:T(8,128)(2,1)} %wk_hbm.1, bf16[512,256]{1,0:T(8,128)(2,1)} %wv_hbm.1, bf16[512,256]{1,0:T(8,128)(2,1)} %wg_hbm.1, ...), custom_call_target="tpu_custom_call" | custom-call | tf_op jit(solution)/shard_map/pallas_call | solution.py:507
  68.0 1.6 %copy.21 = bf16[32,4,512]{2,1,0:T(4,128)(2,1)} copy(bf16[32,4,512]{2,1,0:T(4,128)(2,1)} %get-tuple-element.8) | data formatting | bytes 262144
  69.6 3.1 %copy.22 = f32[32,64,256]{2,1,0:T(8,128)} copy(f32[32,64,256]{2,1,0:T(8,128)} %bitcast.11) | data formatting | bytes 4194304
